TPU v7x, 512 devices: a whole 4x8x8 slice. The times are simulated.
512 devices in a mesh: sp: 64 (over z, y), tp: 4 (over x), dp: 2 (over core).
Axes of the slice: x: 4, y: 8, z: 8, core: 2. Of those that a mesh axis runs over, the one named last changes fastest.
Arguments:
- latent: bfloat16 [2, 8192, 2048], P('dp', ('sp', 'tp')), may hold values from -10 to 10
- condition: bfloat16 [2, 2048], P('dp'), may hold values from -6 to 6
- context: bfloat16 [2, 512, 2048], P('dp', 'sp'), may hold values from -6 to 6
- context_source: bfloat16 [2048], replicated, may hold values from -6 to 6
- mod_weight: bfloat16 [3, 2048, 2048], P(None, 'sp', 'tp'), may hold values from -0.125 to 0.125
- norm_gain: bfloat16 [2048], replicated, may hold values from 0.099609375 to 1.8984375
- w_x: bfloat16 [2048, 2048], P('dp', 'tp'), may hold values from -0.125 to 0.125
- w_b: bfloat16 [2048, 512], P('dp', 'tp'), may hold values from -0.125 to 0.125
- w_c: bfloat16 [2048, 512], P('dp', 'tp'), may hold values from -0.125 to 0.125
- w_z: bfloat16 [2048, 2048], P('dp', 'tp'), may hold values from -0.125 to 0.125
- w_dt: bfloat16 [2, 2048, 32], P(None, 'dp', 'tp'), may hold values from -0.125 to 0.125
- conv_x: bfloat16 [3, 2048], P(None, 'tp'), may hold values from -3.5 to 3.5
- conv_b: bfloat16 [3, 512], P(None, 'tp'), may hold values from -3.5 to 3.5
- conv_c: bfloat16 [3, 512], P(None, 'tp'), may hold values from -3.5 to 3.5
- decay_rate: float32 [2, 32], P(None, 'tp'), may hold values from 0 to 1, as said below
- out_gain: bfloat16 [2048], P('tp'), may hold values from 0.099609375 to 1.8984375
- w_out: bfloat16 [2048, 2048], P(('tp', 'dp')), may hold values from -0.125 to 0.125
Outputs:
- update: bfloat16 [2, 8192, 2048], P('dp', ('sp', 'tp'))
Inputs may be any that keep to these rules, and one draw needn't show every extreme that they name: `decay_rate`: positive rates.
All inputs are finite; a program needn't handle non-finite values.
Results may differ from a plain program's by a relative error of at most 0.014.
Values may be sent and summed in bfloat16 or wider, within the bound.
A program may use at most 128 MiB of HBM per device.

v0:
```python
import functools
import jax
import jax.numpy as jnp
from jax import lax
from jax.sharding import Mesh
from jax.sharding import PartitionSpec as P

STATE = 128
BLOCK = 128
SP = ("sp_0", "sp_1")
SP_TP = ("sp_0", "sp_1", "tp")
EPSILON = 1e-06


def over_axes(x, axes):
    return functools.reduce(lax.psum, axes, x)


def laid_out(tiles, dim):
    tiles = jnp.moveaxis(tiles, 0, dim)
    dims = tiles.shape
    return tiles.reshape(*dims[:dim], dims[dim] * dims[dim + 1], *dims[dim + 2 :])


def sent_to_all(x, axis):
    peers = lax.axis_size(axis)
    return lax.all_to_all(jnp.broadcast_to(x[None], (peers, *x.shape)), axis, 0, 0, tiled=True)


def gather_directly(x, axis, dim):
    return laid_out(sent_to_all(x, axis), dim)


def sent_together(arrays, axis, dim, along):
    ends, at = ([], 0)
    for a in arrays[:-1]:
        at += a.shape[along]
        ends.append(at)
    both = jnp.concatenate(arrays, axis=along)
    return tuple(jnp.split(lax.all_gather(both, axis, axis=dim, tiled=True), ends, axis=along))


def with_halo(x, sides, width):
    for axis, dim in sides:
        peers, length = (lax.axis_size(axis), x.shape[dim])
        up = [(i, (i + 1) % peers) for i in range(peers - 1)]
        down = [(j, i) for i, j in up]
        last = lax.slice_in_dim(x, length - width, length, axis=dim)
        leading = lax.slice_in_dim(x, 0, width, axis=dim)
        before = lax.ppermute(last, axis, up)
        after = lax.ppermute(leading, axis, down)
        x = jnp.concatenate([before, x, after], axis=dim)
    return x


def neutral_like(x, identity):
    return jax.tree.map(
        lambda a, e: jnp.broadcast_to(jnp.asarray(e, a.dtype), a.shape), x, identity
    )


def entering_2(x, axes, combine, identity, reverse):
    before = start = neutral_like(x, identity)
    total = x
    for axis in reversed(axes):
        peers, place = (lax.axis_size(axis), lax.axis_index(axis))
        pieces = jax.tree.map(
            lambda part, kind: lax.all_gather(part.astype(kind), axis),
            total,
            (jnp.bfloat16, jnp.bfloat16),
        )
        inside, total = (start, start)
        for k in reversed(range(peers)) if reverse else range(peers):
            passed = k > place if reverse else k < place
            total = combine(
                total, jax.tree.map(lambda part, own: part[k].astype(own.dtype), pieces, x)
            )
            inside = jax.tree.map(lambda new, old: jnp.where(passed, new, old), total, inside)
        before = combine(inside, before)
    return before


def split_up(x, dim, peers):
    before, after = (x.shape[:dim], x.shape[dim + 1 :])
    return jnp.moveaxis(x.reshape(*before, peers, -1, *after), dim, 0)


def sum_at_owner(x, axis, dim):
    peers = lax.axis_size(axis)
    tiles = lax.all_to_all(split_up(x, dim, peers), axis, 0, 0, tiled=True)
    return jnp.sum(tiles.astype(jnp.float32), axis=0)


def rounded(values):
    return lax.optimization_barrier(values.astype(jnp.bfloat16)).astype(jnp.float32)


def modulated(source, gain_vec, shift_vec, scale_vec):
    values = source.astype(jnp.float32)
    normed = values * lax.rsqrt(jnp.mean(values * values, axis=-1, keepdims=True) + EPSILON)
    return (normed * gain_vec.astype(jnp.float32) * (1.0 + scale_vec) + shift_vec).astype(
        jnp.bfloat16
    )


def convolved(padded, weight, total_rows):
    wide_vals = padded.astype(jnp.float32)
    tap_weights = weight.astype(jnp.float32)
    summed = jnp.zeros((total_rows, wide_vals.shape[1]), jnp.float32)
    for offset in range(weight.shape[0]):
        summed = summed + wide_vals[offset : offset + total_rows] * tap_weights[offset]
    return jax.nn.silu(summed).astype(jnp.bfloat16)


def final_state(x_vals, b_vals, step_size, rate_head, groups):
    total_rows, head_count = step_size.shape
    per_group = head_count // groups
    moved_x = rounded(
        x_vals.reshape(total_rows, head_count, -1).astype(jnp.float32) * step_size[:, :, None]
    )
    running = jnp.cumsum(-rate_head * step_size, axis=0)
    weight = jnp.exp(running[-1:] - running)
    scaled = (moved_x * weight[:, :, None]).reshape(total_rows, groups, per_group, -1)
    b_wide = b_vals.reshape(total_rows, groups, -1).astype(jnp.float32)
    ctx_state = jnp.einsum("sgn,sghp->ghpn", b_wide, scaled)
    return (ctx_state, running[-1].reshape(groups, per_group))


def combine_states(earlier, later_part):
    return (
        earlier[0] + later_part[0],
        earlier[1] * jnp.exp(later_part[0])[:, :, None, None] + later_part[1],
    )


def direction_terms(x_vals, b_vals, c_vals, step_size, rate_head, groups):
    total_rows, head_count = step_size.shape
    per_group = head_count // groups
    blocks = total_rows // BLOCK
    moved_x = (
        x_vals.reshape(total_rows, head_count, -1).astype(jnp.float32) * step_size[:, :, None]
    ).astype(jnp.bfloat16)
    head_dim = moved_x.shape[2]
    x_blocks = moved_x.reshape(blocks, BLOCK, groups, per_group, head_dim)
    b_blocks = b_vals.reshape(blocks, BLOCK, groups, -1)
    c_blocks = c_vals.reshape(blocks, BLOCK, groups, -1)
    running = jnp.cumsum((-rate_head * step_size).reshape(blocks, BLOCK, head_count), axis=1)
    across = jnp.swapaxes(running, 1, 2)
    spread = across[:, :, :, None] - across[:, :, None, :]
    lower_part = lax.broadcasted_iota(jnp.int32, (BLOCK, BLOCK), 0) >= lax.broadcasted_iota(
        jnp.int32, (BLOCK, BLOCK), 1
    )
    decay_mask = jnp.where(lower_part, jnp.exp(jnp.minimum(spread, 0.0)), 0.0).reshape(
        blocks, groups, per_group, BLOCK, BLOCK
    )
    scores = jnp.einsum("clgn,csgn->cgls", c_blocks, b_blocks, preferred_element_type=jnp.float32)
    weights = (scores[:, :, None] * decay_mask).astype(jnp.bfloat16)
    inside = jnp.einsum("cghls,csghp->clghp", weights, x_blocks, preferred_element_type=jnp.float32)
    to_end = jnp.exp(running[:, -1:, :] - running).reshape(blocks, BLOCK, groups, per_group, 1)
    x_end = (x_blocks.astype(jnp.float32) * to_end).astype(jnp.bfloat16)
    fresh_state = jnp.einsum(
        "csgn,csghp->cghpn", b_blocks, x_end, preferred_element_type=jnp.float32
    )
    totals = running[:, -1, :].reshape(blocks, groups, per_group)

    def advance(carried_in, inputs):
        return (carried_in * jnp.exp(inputs[1])[:, :, None, None] + inputs[0], carried_in)

    ending, before = lax.scan(
        advance, jnp.zeros(fresh_state.shape[1:], jnp.float32), (fresh_state, totals)
    )
    return (inside, before, ending, totals, running, c_blocks)


def direction_output(terms, incoming):
    inside, before, ending, totals, running, c_blocks = terms
    blocks, length, groups, per_group, head_dim = inside.shape
    offset_sum = jnp.cumsum(totals, axis=0) - totals
    entering = before + jnp.exp(offset_sum)[:, :, :, None, None] * incoming[None]
    carried = jnp.einsum(
        "clgn,cghpn->clghp",
        c_blocks,
        entering.astype(jnp.bfloat16),
        preferred_element_type=jnp.float32,
    )
    growth = jnp.exp(running).reshape(blocks, length, groups, per_group, 1)
    return (inside + growth * carried).reshape(blocks * length, -1)


def shards(
    latent,
    condition,
    context,
    context_source,
    mod_weight,
    norm_gain,
    w_x,
    w_b,
    w_c,
    w_z,
    w_dt,
    conv_x,
    conv_b,
    conv_c,
    decay_rate,
    out_gain,
    w_out,
):
    row_count = mod_weight.shape[1]
    activations = jnp.stack(
        [
            jax.nn.silu(condition[0].astype(jnp.float32)),
            jax.nn.silu(context_source.astype(jnp.float32)),
        ]
    ).astype(jnp.bfloat16)
    own_rows = lax.dynamic_slice_in_dim(activations, lax.axis_index(SP) * row_count, row_count, 1)
    partial_value = jnp.einsum(
        "ar,krc->kac", own_rows, mod_weight, preferred_element_type=jnp.float32
    )
    summed = over_axes(partial_value, SP)
    mod_vectors = gather_directly(summed, "tp", 2)
    full_x, full_b, full_c, full_z, full_fwd, full_bwd, full_out = (
        *sent_together((w_x, w_b, w_c, w_z, w_dt[0], w_dt[1]), "dp", 0, 1),
        lax.all_gather(w_out, "dp", axis=0, tiled=True),
    )
    inner_cols = full_x.shape[1]
    gn_cols = full_b.shape[1]
    head_count = full_fwd.shape[1]
    groups = gn_cols // STATE
    mixed_cols = inner_cols + gn_cols
    reach_rows = conv_x.shape[0] // 2
    rate_fwd = decay_rate[0]
    rate_bwd = decay_rate[1]
    all_weights = jnp.concatenate([full_x, full_b, full_c, full_fwd, full_bwd, full_z], axis=1)
    ctx_weight = jnp.concatenate([full_x, full_b, full_fwd, full_bwd], axis=1)
    taps_all = jnp.concatenate([conv_x, conv_b, conv_c], axis=1)
    ctx_taps = jnp.concatenate([conv_x, conv_b], axis=1)
    ctx_rows = modulated(context[0], norm_gain, mod_vectors[0, 1], mod_vectors[1, 1])
    own_features = jnp.dot(ctx_rows, ctx_weight, preferred_element_type=jnp.float32).astype(
        jnp.bfloat16
    )
    features = gather_directly(own_features, SP, 0)
    total_rows = features.shape[0]
    padded = jnp.pad(features[:, :mixed_cols], ((reach_rows, reach_rows), (0, 0)))
    smoothed = convolved(padded, ctx_taps, total_rows)
    step_size = jax.nn.softplus(features[:, mixed_cols:].astype(jnp.float32))
    ctx_x = smoothed[:, :inner_cols]
    ctx_b = smoothed[:, inner_cols:]
    state_fwd, _ = final_state(ctx_x, ctx_b, step_size[:, :head_count], rate_fwd, groups)
    state_bwd, _ = final_state(
        jnp.flip(ctx_x, 0),
        jnp.flip(ctx_b, 0),
        jnp.flip(step_size[:, head_count:], 0),
        rate_bwd,
        groups,
    )
    latent_rows = modulated(latent[0], norm_gain, mod_vectors[0, 0], mod_vectors[1, 0])
    features = jnp.dot(
        gather_directly(latent_rows, "tp", 0), all_weights, preferred_element_type=jnp.float32
    ).astype(jnp.bfloat16)
    total_rows = features.shape[0]
    padded = with_halo(features[:, : mixed_cols + gn_cols], ((SP, 0),), reach_rows)
    smoothed = convolved(padded, taps_all, total_rows)
    x_vals = smoothed[:, :inner_cols]
    b_vals = smoothed[:, inner_cols:mixed_cols]
    c_vals = smoothed[:, mixed_cols:]
    base_col = mixed_cols + gn_cols
    step_size = jax.nn.softplus(
        features[:, base_col : base_col + 2 * head_count].astype(jnp.float32)
    )
    gate_in = features[:, base_col + 2 * head_count :]
    forward_terms = direction_terms(
        x_vals, b_vals, c_vals, step_size[:, :head_count], rate_fwd, groups
    )
    backward_terms = direction_terms(
        jnp.flip(x_vals, 0),
        jnp.flip(b_vals, 0),
        jnp.flip(c_vals, 0),
        jnp.flip(step_size[:, head_count:], 0),
        rate_bwd,
        groups,
    )
    fwd_total = jnp.sum(forward_terms[3], axis=0)
    bwd_total = jnp.sum(backward_terms[3], axis=0)
    empty = (jnp.zeros_like(fwd_total), jnp.zeros_like(forward_terms[2]))
    prefix_decay, prefix_state = entering_2(
        (fwd_total, forward_terms[2]), SP, combine_states, empty, False
    )
    suffix_decay, suffix_state = entering_2(
        (bwd_total, backward_terms[2]), SP, combine_states, empty, True
    )
    out_fwd = direction_output(
        forward_terms, prefix_state + jnp.exp(prefix_decay)[:, :, None, None] * state_fwd
    )
    out_bwd = jnp.flip(
        direction_output(
            backward_terms, suffix_state + jnp.exp(suffix_decay)[:, :, None, None] * state_bwd
        ),
        0,
    )
    gated = (out_fwd + out_bwd) * jax.nn.silu(gate_in.astype(jnp.float32))
    grouped = gated.reshape(total_rows, groups, -1)
    normed = (
        grouped
        * lax.rsqrt(jnp.mean(grouped * grouped, axis=-1, keepdims=True) + EPSILON)
        * out_gain.reshape(groups, -1).astype(jnp.float32)
    )
    normed_out = normed.reshape(total_rows, -1).astype(jnp.bfloat16)
    mixed = sum_at_owner(
        jnp.dot(normed_out, full_out, preferred_element_type=jnp.float32).astype(jnp.bfloat16),
        "tp",
        0,
    )
    return (mod_vectors[2, 0] * mixed).astype(jnp.bfloat16)[None]


def solution(mesh):
    torus = Mesh(
        mesh.devices.reshape(8, 8, mesh.shape["tp"], mesh.shape["dp"]), ("sp_0", "sp_1", "tp", "dp")
    )
    placed = (
        P("dp", SP_TP, None),
        P("dp", None),
        P("dp", SP, None),
        P(),
        P(None, SP, "tp"),
        P(),
        P("dp", "tp"),
        P("dp", "tp"),
        P("dp", "tp"),
        P("dp", "tp"),
        P(None, "dp", "tp"),
        P(None, "tp"),
        P(None, "tp"),
        P(None, "tp"),
        P(None, "tp"),
        P("tp"),
        P(("tp", "dp"), None),
    )
    return jax.shard_map(
        shards, mesh=torus, in_specs=placed, out_specs=P("dp", SP_TP, None), check_vma=False
    )
```

profile of v0, /device:TPU:1, one launch (start us, length us, event | category | flops | bytes accessed | tf_op | source)
XLA Modules:
  0.0 347.1 jit_solution(8498954441574411239)
XLA Ops:
  7.7 5.4 %concatenate.20 = bf16[1024,1296]{1,0:T(8,128)(2,1)} concatenate(bf16[1024,512]{1,0:T(8,128)(2,1)} %param.23, bf16[1024,128]{1,0:T(8,128)(2,1)} %param.24, bf16[1024,128]{1,0:T(8,128)(2,1)} %param.25, bf16[1024,512]{1,0:T(8,128)(2,1)} %param.26, bf16[1024,8]{1,0:T(8,128)(2,1)S(1)} %copy.97, bf16[1024,8]{1,0:T(8,128)(2,1)S(1)} %copy.98), dimensions={1} | concatenate | bytes 5308416 | tf_op jit(solution)/shard_map/concatenate | solution.py:39
  14.0 29.8 %psum.14 = f32[3,2,512]{2,1,0:T(2,128)S(1)} all-reduce(f32[3,2,512]{2,1,0:T(2,128)S(1)} %convolution_bitcast_fusion.4), channel_id=1, replica_groups=mesh['sp_0'=8,'sp_1'=8,'tp'=4,'dp'=2] {'sp_0'}, use_global_device_ids=true, to_apply=%region_0.1 | all-reduce | flops 3072 | bytes 24576 | tf_op jit(solution)/shard_map/psum | solution.py:16
  43.8 23.1 %psum.15 = f32[3,2,512]{2,1,0:T(2,128)S(1)} all-reduce(f32[3,2,512]{2,1,0:T(2,128)S(1)} %psum.14), channel_id=1, replica_groups=mesh['sp_0'=8,'sp_1'=8,'tp'=4,'dp'=2] {'sp_1'}, use_global_device_ids=true, to_apply=%region_1.2 | all-reduce | flops 3072 | bytes 24576 | tf_op jit(solution)/shard_map/psum | solution.py:16
  67.5 4.0 %all-to-all-start = ((f32[4,3,2,512]{3,2,1,0:T(2,128)}), f32[4,3,2,512]{3,2,1,0:T(2,128)S(1)}, u32[]{:S(2)}, u32[]{:S(2)}) async-start(f32[4,3,2,512]{3,2,1,0:T(2,128)} %broadcast_in_dim.22), calls=%async_computation | async-start | bytes 98304 | tf_op jit(solution)/shard_map/all_to_all | solution.py:27
  71.7 4.2 %all-to-all-done = f32[4,3,2,512]{3,2,1,0:T(2,128)S(1)} async-done(((f32[4,3,2,512]{3,2,1,0:T(2,128)}), f32[4,3,2,512]{3,2,1,0:T(2,128)S(1)}, u32[]{:S(2)}, u32[]{:S(2)}) %all-to-all-start) | async-done | bytes 49184 | tf_op jit(solution)/shard_map/all_to_all | solution.py:27
  77.5 4.1 %all-to-all-start.1 = ((bf16[4,32,2048]{2,1,0:T(8,128)(2,1)}), bf16[4,32,2048]{2,1,0:T(8,128)(2,1)}, u32[]{:S(2)}, u32[]{:S(2)}) async-start(bf16[4,32,2048]{2,1,0:T(8,128)(2,1)} %broadcast_in_dim.24), calls=%async_computation.1 | async-start | bytes 1048576 | tf_op jit(solution)/shard_map/all_to_all | solution.py:27
  81.9 1.9 split.19
  83.8 3.1 split.20
  86.8 2.1 split.18
  88.9 9.4 %concatenate.21 = bf16[2048,1296]{1,0:T(8,128)(2,1)} concatenate(bf16[2048,768]{1,0:T(8,128)(2,1)S(1)} %split.18, bf16[2048,16]{1,0:T(8,128)(2,1)} %split.19, bf16[2048,512]{1,0:T(8,128)(2,1)} %split.20), dimensions={1} | concatenate | bytes 10616832 | tf_op jit(solution)/shard_map/concatenate | solution.py:234
  98.3 5.1 %convolution_convert_fusion.1 = bf16[128,1296]{0,1:T(8,128)(2,1)S(1)} fusion(bf16[128,2048]{1,0:T(8,128)(2,1)} %bitcast.7, bf16[2048,1296]{1,0:T(8,128)(2,1)} %concatenate.21), kind=kOutput, calls=%fused_computation.5 | convolution fusion | flops 679643136 | bytes 6164480 | tf_op jit(solution)/shard_map/dot_general | solution.py:258
  104.8 1.7 collective-permute-start
  109.1 3.8 %collective-permute-done.1 = bf16[1,768]{0,1:T(8,128)(2,1)S(1)} collective-permute-done((bf16[1,768]{0,1:T(8,128)(2,1)S(1)}, bf16[1,768]{0,1:T(8,128)(2,1)S(1)}, u32[]{:S(2)}, u32[]{:S(2)}) %collective-permute-start.1) | collective-permute-done | bytes 1568 | tf_op jit(solution)/shard_map/ppermute | solution.py:51
  118.5 13.1 %all_gather.48 = bf16[8,1,8]{2,1,0:T(2,128)(2,1)S(1)} all-gather(bf16[1,1,8]{2,1,0:T(2,128)(2,1)S(1)} %slice.999), channel_id=1, replica_groups=mesh['sp_0'=8,'sp_1'=8,'tp'=4,'dp'=2] {'sp_1'}, dimensions={0}, use_global_device_ids=true | all-gather | bytes 144 | tf_op jit(solution)/shard_map/all_gather | solution.py:68
  131.7 35.6 %all-gather.19.cloned.1.call-done = bf16[64,64,128]{2,1,0:T(8,128)(2,1)} async-done(((bf16[8,64,128]{2,1,0:T(8,128)(2,1)}), bf16[64,64,128]{2,1,0:T(8,128)(2,1)}) %all-gather.19.cloned.1.call-update) | async-done | bytes 1048592 | tf_op jit(solution)/shard_map/all_gather | solution.py:68
  167.2 2.3 fusion.159
  169.6 11.2 %all_gather.43 = bf16[8,1,8]{2,1,0:T(2,128)(2,1)S(1)} all-gather(bf16[1,1,8]{2,1,0:T(2,128)(2,1)S(1)} %slice.1000), channel_id=1, replica_groups=mesh['sp_0'=8,'sp_1'=8,'tp'=4,'dp'=2] {'sp_1'}, dimensions={0}, use_global_device_ids=true | all-gather | bytes 144 | tf_op jit(solution)/shard_map/all_gather | solution.py:68
  180.9 28.2 %all-gather.17.cloned.1.call-done = bf16[64,64,128]{2,1,0:T(8,128)(2,1)} async-done(((bf16[8,64,128]{2,1,0:T(8,128)(2,1)}), bf16[64,64,128]{2,1,0:T(8,128)(2,1)}) %all-gather.17.cloned.1.call-update) | async-done | bytes 1048592 | tf_op jit(solution)/shard_map/all_gather | solution.py:68
  209.1 2.2 fusion.160
  213.4 13.5 %all_gather.49 = bf16[8,1,8]{2,1,0:T(2,128)(2,1)S(1)} all-gather(bf16[1,1,8]{2,1,0:T(2,128)(2,1)S(1)} %get-tuple-element.103), channel_id=1, replica_groups=mesh['sp_0'=8,'sp_1'=8,'tp'=4,'dp'=2] {'sp_0'}, dimensions={0}, use_global_device_ids=true | all-gather | bytes 144 | tf_op jit(solution)/shard_map/all_gather | solution.py:68
  227.6 10.5 %all_gather.44 = bf16[8,1,8]{2,1,0:T(2,128)(2,1)S(1)} all-gather(bf16[1,1,8]{2,1,0:T(2,128)(2,1)S(1)} %get-tuple-element.83), channel_id=1, replica_groups=mesh['sp_0'=8,'sp_1'=8,'tp'=4,'dp'=2] {'sp_0'}, dimensions={0}, use_global_device_ids=true | all-gather | bytes 144 | tf_op jit(solution)/shard_map/all_gather | solution.py:68
  238.8 1.7 slice-done
  242.2 8.2 %all-to-all-start.2 = ((bf16[64,8,656]{2,1,0:T(8,128)(2,1)}), bf16[64,8,656]{2,1,0:T(8,128)(2,1)S(1)}, u32[]{:S(2)}, u32[]{:S(2)}) async-start(bf16[64,8,656]{2,1,0:T(8,128)(2,1)} %broadcast_in_dim.26), calls=%async_computation.2 | async-start | bytes 1572864 | tf_op jit(solution)/shard_map/all_to_all | solution.py:27
  255.4 11.4 %all-to-all-done.2 = bf16[64,8,656]{2,1,0:T(8,128)(2,1)S(1)} async-done(((bf16[64,8,656]{2,1,0:T(8,128)(2,1)}), bf16[64,8,656]{2,1,0:T(8,128)(2,1)S(1)}, u32[]{:S(2)}, u32[]{:S(2)}) %all-to-all-start.2) | async-done | bytes 671776 | tf_op jit(solution)/shard_map/all_to_all | solution.py:27
  275.5 1.7 multiply_convert_fusion.2
  277.3 6.3 %rev.35 = bf16[512,512]{1,0:T(8,128)(2,1)S(1)} reverse(bf16[512,512]{1,0:T(8,128)(2,1)} %get-tuple-element.48), dimensions={0} | reverse | bytes 1048576 | tf_op jit(solution)/shard_map/jit(_flip)/rev | solution.py:251
  284.7 3.3 fusion.13
  289.7 10.8 %all-gather.11.cloned.1.call-done = bf16[8,1,8,64,128]{4,3,2,1,0:T(8,128)(2,1)} async-done(((bf16[1,1,8,64,128]{4,3,2,1,0:T(8,128)(2,1)}), bf16[8,1,8,64,128]{4,3,2,1,0:T(8,128)(2,1)}) %all-gather.11.cloned.1.call-update) | async-done | bytes 1048592 | tf_op jit(solution)/shard_map/all_gather | solution.py:68
  300.8 2.6 fusion.12
  303.9 21.7 %all-gather.15.cloned.1.call-done = bf16[512,2048]{1,0:T(8,128)(2,1)} async-done(((bf16[256,2048]{1,0:T(8,128)(2,1)}), bf16[512,2048]{1,0:T(8,128)(2,1)}) %all-gather.15.cloned.1.call-update) | async-done | bytes 2097168 | tf_op jit(solution)/shard_map/all_gather | solution.py:224
  325.5 2.1 convolution_convert_fusion
  327.7 11.9 %all_to_all.20 = bf16[4,32,2048]{2,1,0:T(8,128)(2,1)S(1)} all-to-all(bf16[4,32,2048]{2,1,0:T(8,128)(2,1)S(1)} %bitcast.494), channel_id=1, replica_groups=mesh['sp_0'=8,'sp_1'=8,'tp'=4,'dp'=2] {'tp'}, dimensions={0} | all-to-all | bytes 1048576 | tf_op jit(solution)/shard_map/all_to_all | solution.py:90
  (287 shorter events, 36.3 us)
Async XLA Ops:
  6.5 75.3 %all-gather.9.cloned.1.call-start = ((), (), s32[]{:S(2)}) async-start(), calls=%async_computation.4 | async-start | bytes 8650752 | tf_op jit(solution)/shard_map/all_gather | solution.py:40
  13.1 58.5 %copy-start.3 = (bf16[1,32,2048]{2,1,0:T(8,128)(2,1)S(1)}, bf16[1,32,2048]{2,1,0:T(8,128)(2,1)}, u32[]{:S(2)}) copy-start(bf16[1,32,2048]{2,1,0:T(8,128)(2,1)} %param.17) | copy-start | bytes 393220
  13.1 58.6 %copy-start.25 = (bf16[2048]{0:T(1024)(128)(2,1)S(1)}, bf16[2048]{0:T(1024)(128)(2,1)}, u32[]{:S(2)}) copy-start(bf16[2048]{0:T(1024)(128)(2,1)} %param.22) | copy-start | bytes 12292
  13.1 68.6 %copy-start.15 = (bf16[3,512]{1,0:T(4,128)(2,1)S(1)}, bf16[3,512]{1,0:T(4,128)(2,1)}, u32[]{:S(2)}) copy-start(bf16[3,512]{1,0:T(4,128)(2,1)} %param.28) | copy-start | bytes 9220
  13.1 68.6 %copy-start.30 = (bf16[3,128]{1,0:T(4,128)(2,1)S(1)}, bf16[3,128]{1,0:T(4,128)(2,1)}, u32[]{:S(2)}) copy-start(bf16[3,128]{1,0:T(4,128)(2,1)} %param.29) | copy-start | bytes 2308
  13.1 68.6 %copy-start.66 = (bf16[3,128]{1,0:T(4,128)(2,1)S(1)}, bf16[3,128]{1,0:T(4,128)(2,1)}, u32[]{:S(2)}) copy-start(bf16[3,128]{1,0:T(4,128)(2,1)} %param.30) | copy-start | bytes 2308
  13.1 68.7 %copy-start.68 = (f32[2,8]{1,0:T(2,128)S(1)}, f32[2,8]{1,0:T(2,128)}, u32[]{:S(2)}) copy-start(f32[2,8]{1,0:T(2,128)} %param.31) | copy-start | bytes 196
  67.5 8.4 %all-to-all-start = ((f32[4,3,2,512]{3,2,1,0:T(2,128)}), f32[4,3,2,512]{3,2,1,0:T(2,128)S(1)}, u32[]{:S(2)}, u32[]{:S(2)}) async-start(f32[4,3,2,512]{3,2,1,0:T(2,128)} %broadcast_in_dim.22), calls=%async_computation | async-start | bytes 98304 | tf_op jit(solution)/shard_map/all_to_all | solution.py:27
  77.5 20.8 %all-to-all-start.1 = ((bf16[4,32,2048]{2,1,0:T(8,128)(2,1)}), bf16[4,32,2048]{2,1,0:T(8,128)(2,1)}, u32[]{:S(2)}, u32[]{:S(2)}) async-start(bf16[4,32,2048]{2,1,0:T(8,128)(2,1)} %broadcast_in_dim.24), calls=%async_computation.1 | async-start | bytes 1048576 | tf_op jit(solution)/shard_map/all_to_all | solution.py:27
  81.7 85.5 %all-gather.19.cloned.1.call-start = ((), (), s32[]{:S(2)}) async-start(), calls=%async_computation.9 | async-start | bytes 1179648 | tf_op jit(solution)/shard_map/all_gather | solution.py:68
  104.8 4.3 %collective-permute-start = (bf16[1,768]{0,1:T(8,128)(2,1)S(1)}, bf16[1,768]{0,1:T(8,128)(2,1)S(1)}, u32[]{:S(2)}, u32[]{:S(2)}) collective-permute-start(bf16[1,768]{0,1:T(8,128)(2,1)S(1)} %get-tuple-element.49), channel_id=1, source_target_pairs={{0,8},{8,16},{16,24},{24,32},{32,40},{40,48},{48,56},{56,64},{64,7... | collective-permute-start | bytes 4616 | tf_op jit(solution)/shard_map/ppermute | solution.py:50
  106.5 6.4 %collective-permute-start.1 = (bf16[1,768]{0,1:T(8,128)(2,1)S(1)}, bf16[1,768]{0,1:T(8,128)(2,1)S(1)}, u32[]{:S(2)}, u32[]{:S(2)}) collective-permute-start(bf16[1,768]{0,1:T(8,128)(2,1)S(1)} %get-tuple-element.50), channel_id=1, source_target_pairs={{8,0},{16,8},{24,16},{32,24},{40,32},{48,40},{56,48},{64,56},{72,6... | collective-permute-start | bytes 4616 | tf_op jit(solution)/shard_map/ppermute | solution.py:51
  115.9 93.1 %all-gather.17.cloned.1.call-start = ((), (), s32[]{:S(2)}) async-start(), calls=%async_computation.8 | async-start | bytes 1179648 | tf_op jit(solution)/shard_map/all_gather | solution.py:68
  117.5 94.5 %copy-start.16 = (bf16[3,512]{1,0:T(4,128)(2,1)S(1)}, bf16[3,512]{1,0:T(4,128)(2,1)}, u32[]{:S(2)}) copy-start(bf16[3,512]{1,0:T(4,128)(2,1)} %param.28) | copy-start | bytes 9220
  117.6 94.5 %copy-start.31 = (bf16[3,128]{1,0:T(4,128)(2,1)S(1)}, bf16[3,128]{1,0:T(4,128)(2,1)}, u32[]{:S(2)}) copy-start(bf16[3,128]{1,0:T(4,128)(2,1)} %param.29) | copy-start | bytes 2308
  117.6 95.1 %copy-start.11 = (bf16[1,8,2048]{2,1,0:T(8,128)(2,1)S(1)}, bf16[1,8,2048]{2,1,0:T(8,128)(2,1)}, u32[]{:S(2)}) copy-start(bf16[1,8,2048]{2,1,0:T(8,128)(2,1)} %param.19) | copy-start | bytes 98308
  117.6 95.2 %copy-start.67 = (bf16[512]{0:T(512)(128)(2,1)S(1)}, bf16[512]{0:T(512)(128)(2,1)}, u32[]{:S(2)}) copy-start(bf16[512]{0:T(512)(128)(2,1)} %param.32) | copy-start | bytes 3076
  118.5 165.9 %all-gather.13.cloned.1.call-start = ((), (), s32[]{:S(2)}) async-start(), calls=%async_computation.6 | async-start | bytes 1179648 | tf_op jit(solution)/shard_map/all_gather | solution.py:68
  131.6 38.0 %copy-start.51 = (f32[8]{0:T(128)}, f32[8]{0:T(128)S(1)}, u32[]{:S(2)}) copy-start(f32[8]{0:T(128)S(1)} %get-tuple-element.105) | copy-start | bytes 100
  131.6 38.0 %copy-start.53 = (f32[8]{0:T(128)}, f32[8]{0:T(128)S(1)}, u32[]{:S(2)}) copy-start(f32[8]{0:T(128)S(1)} %get-tuple-element.106) | copy-start | bytes 100
  131.6 38.0 %copy-start.55 = (f32[8]{0:T(128)}, f32[8]{0:T(128)S(1)}, u32[]{:S(2)}) copy-start(f32[8]{0:T(128)S(1)} %get-tuple-element.107) | copy-start | bytes 100
  131.6 38.0 %copy-start.57 = (f32[8]{0:T(128)}, f32[8]{0:T(128)S(1)}, u32[]{:S(2)}) copy-start(f32[8]{0:T(128)S(1)} %get-tuple-element.108) | copy-start | bytes 100
  131.6 38.0 %copy-start.59 = (f32[8]{0:T(128)}, f32[8]{0:T(128)S(1)}, u32[]{:S(2)}) copy-start(f32[8]{0:T(128)S(1)} %get-tuple-element.109) | copy-start | bytes 100
  169.5 131.0 %all-gather.11.cloned.1.call-start = ((), (), s32[]{:S(2)}) async-start(), calls=%async_computation.5 | async-start | bytes 1179648 | tf_op jit(solution)/shard_map/all_gather | solution.py:68
  180.8 57.9 %copy-start.37 = (f32[8]{0:T(128)}, f32[8]{0:T(128)S(1)}, u32[]{:S(2)}) copy-start(f32[8]{0:T(128)S(1)} %get-tuple-element.86) | copy-start | bytes 100
  180.8 57.9 %copy-start.39 = (f32[8]{0:T(128)}, f32[8]{0:T(128)S(1)}, u32[]{:S(2)}) copy-start(f32[8]{0:T(128)S(1)} %get-tuple-element.87) | copy-start | bytes 100
  180.9 57.9 %copy-start.41 = (f32[8]{0:T(128)}, f32[8]{0:T(128)S(1)}, u32[]{:S(2)}) copy-start(f32[8]{0:T(128)S(1)} %get-tuple-element.88) | copy-start | bytes 100
  180.9 57.9 %copy-start.43 = (f32[8]{0:T(128)}, f32[8]{0:T(128)S(1)}, u32[]{:S(2)}) copy-start(f32[8]{0:T(128)S(1)} %get-tuple-element.89) | copy-start | bytes 100
  180.9 57.9 %copy-start.45 = (f32[8]{0:T(128)}, f32[8]{0:T(128)S(1)}, u32[]{:S(2)}) copy-start(f32[8]{0:T(128)S(1)} %get-tuple-element.90) | copy-start | bytes 100
  180.9 57.9 %copy-start.47 = (f32[8]{0:T(128)}, f32[8]{0:T(128)S(1)}, u32[]{:S(2)}) copy-start(f32[8]{0:T(128)S(1)} %get-tuple-element.91) | copy-start | bytes 100
  211.4 114.2 %all-gather.15.cloned.1.call-start = ((), (), s32[]{:S(2)}) async-start(), calls=%async_computation.7 | async-start | bytes 3145728 | tf_op jit(solution)/shard_map/all_gather | solution.py:224
  242.2 24.7 %all-to-all-start.2 = ((bf16[64,8,656]{2,1,0:T(8,128)(2,1)}), bf16[64,8,656]{2,1,0:T(8,128)(2,1)S(1)}, u32[]{:S(2)}, u32[]{:S(2)}) async-start(bf16[64,8,656]{2,1,0:T(8,128)(2,1)} %broadcast_in_dim.26), calls=%async_computation.2 | async-start | bytes 1572864 | tf_op jit(solution)/shard_map/all_to_all | solution.py:27
  (63 other events, 756.4 us)
Sparse Core Ops, SparseCore 0:
  13.3 31.0 all-gather.8
  116.1 51.1 all-gather.18
  169.3 39.7 all-gather.16
  211.0 41.0 all-gather.12
  254.0 46.4 all-gather.10
  302.5 22.9 all-gather.14
where the time goes:
time: 349 us; the launch traced here: 347 us
  waiting for transfers between devices  117 us (34%)
  blocking collectives  113 us (32%)
  local copies, waits for them, and re-layouts  40.7 us (12%)
  other arithmetic  23 us (7%)
  starting transfers between devices  19.6 us (6%)
  matrix products  18.9 us (5%)
  between operations  15 us (4%)
    all_gather x4, waiting for transfers between devices, entering_2(): lax.all_gather(part.astype(kind), axis)  74.5 us
    psum x2, blocking collectives, over_axes(): return functools.reduce(lax.psum, axes, x)  52.9 us
    all_gather x4, blocking collectives, entering_2(): lax.all_gather(part.astype(kind), axis)  48.2 us
    all_gather x1, waiting for transfers between devices, shards(): lax.all_gather(w_out, 'dp', axis=0, tiled=True)  21.7 us
    all_to_all x3, starting transfers between devices, sent_to_all(): lax.all_to_all(jnp.broadcast_to(x[None], (peers, *x.shape)), axis, 0, 0,...  16.4 us
    all_to_all x3, waiting for transfers between devices, sent_to_all(): lax.all_to_all(jnp.broadcast_to(x[None], (peers, *x.shape)), axis, 0, 0,...  15.7 us
    all_to_all x1, blocking collectives, sum_at_owner(): tiles = lax.all_to_all(split_up(x, dim, peers), axis, 0, 0, tiled=True)  11.9 us
    concatenate x1, local copies, waits for them, and re-layouts, shards(): jnp.concatenate([full_x, full_b, full_c, full_fwd, full_bwd, full_z], axi...  9.42 us
  transfers between devices with their start and end apart: 11, of which 8 were waited for; matrix products, arithmetic and copies ran while one was open for 18% of the time, Pallas kernels for 0%

commit v1 on v0

--- a/solution.py
+++ b/solution.py
@@ -219,9 +219,16 @@
     )
     summed = over_axes(partial_value, SP)
     mod_vectors = gather_directly(summed, "tp", 2)
+
+    def edit_weights(local_block):
+        clean = jnp.stack([local_block for _ in range(jax.lax.axis_size("dp"))], axis=0)
+        vec_out = jax.lax.all_to_all(clean, axis_name="dp", concat_axis=0, split_axis=0)
+        then = jnp.concatenate(vec_out, 0)
+        return then
+
     full_x, full_b, full_c, full_z, full_fwd, full_bwd, full_out = (
         *sent_together((w_x, w_b, w_c, w_z, w_dt[0], w_dt[1]), "dp", 0, 1),
-        lax.all_gather(w_out, "dp", axis=0, tiled=True),
+        edit_weights(w_out),
     )
     inner_cols = full_x.shape[1]
     gn_cols = full_b.shape[1]

time: 349 us -> 360 us (1.032)
  the two profiles are of different devices: /device:TPU:1 before, /device:TPU:8 now
where the time goes in v1:
time: 360 us; the launch traced here: 358 us
  blocking collectives  147 us (41%)
  waiting for transfers between devices  75.5 us (21%)
  local copies, waits for them, and re-layouts  46 us (13%)
  starting transfers between devices  28.9 us (8%)
  other arithmetic  27.3 us (8%)
  matrix products  19.5 us (5%)
  between operations  13.9 us (4%)
    all_gather x4, blocking collectives, entering_2(): lax.all_gather(part.astype(kind), axis)  70.7 us
    all_gather x4, waiting for transfers between devices, entering_2(): lax.all_gather(part.astype(kind), axis)  66.2 us
    psum x2, blocking collectives, over_axes(): return functools.reduce(lax.psum, axes, x)  64.3 us
    all_to_all x3, starting transfers between devices, sent_to_all(): lax.all_to_all(jnp.broadcast_to(x[None], (peers, *x.shape)), axis, 0, 0,...  18.9 us
    all_to_all x1, blocking collectives, sum_at_owner(): tiles = lax.all_to_all(split_up(x, dim, peers), axis, 0, 0, tiled=True)  12.1 us
    concatenate x1, local copies, waits for them, and re-layouts, shards(): jnp.concatenate([full_x, full_b, full_c, full_fwd, full_bwd, full_z], axi...  9.42 us
    split x5, local copies, waits for them, and re-layouts, sent_together(): jnp.split(lax.all_gather(both, axis, axis=dim, tiled=True), ends, axis=al...  8.75 us
    rev x1, local copies, waits for them, and re-layouts, shards(): jnp.flip(ctx_x, 0)  8.31 us
  transfers between devices with their start and end apart: 11, of which 5 were waited for; matrix products, arithmetic and copies ran while one was open for 20% of the time, Pallas kernels for 0%

profile of v1, /device:TPU:8, one launch (start us, length us, event | category | flops | bytes accessed | tf_op | source)
XLA Modules:
  0.0 358.2 jit_solution(13981238978804822432)
XLA Ops:
  7.7 5.4 %concatenate.20 = bf16[1024,1296]{1,0:T(8,128)(2,1)} concatenate(bf16[1024,512]{1,0:T(8,128)(2,1)} %param.23, bf16[1024,128]{1,0:T(8,128)(2,1)} %param.24, bf16[1024,128]{1,0:T(8,128)(2,1)} %param.25, bf16[1024,512]{1,0:T(8,128)(2,1)} %param.26, bf16[1024,8]{1,0:T(8,128)(2,1)S(1)} %copy.97, bf16[1024,8]{1,0:T(8,128)(2,1)S(1)} %copy.98), dimensions={1} | concatenate | bytes 5308416 | tf_op jit(solution)/shard_map/concatenate | solution.py:39
  14.0 35.9 %psum.14 = f32[3,2,512]{2,1,0:T(2,128)S(1)} all-reduce(f32[3,2,512]{2,1,0:T(2,128)S(1)} %convolution_bitcast_fusion.4), channel_id=1, replica_groups=mesh['sp_0'=8,'sp_1'=8,'tp'=4,'dp'=2] {'sp_0'}, use_global_device_ids=true, to_apply=%region_0.1 | all-reduce | flops 3072 | bytes 24576 | tf_op jit(solution)/shard_map/psum | solution.py:16
  49.9 28.4 %psum.15 = f32[3,2,512]{2,1,0:T(2,128)S(1)} all-reduce(f32[3,2,512]{2,1,0:T(2,128)S(1)} %psum.14), channel_id=1, replica_groups=mesh['sp_0'=8,'sp_1'=8,'tp'=4,'dp'=2] {'sp_1'}, use_global_device_ids=true, to_apply=%region_1.2 | all-reduce | flops 3072 | bytes 24576 | tf_op jit(solution)/shard_map/psum | solution.py:16
  79.0 4.3 %all-to-all-start = ((f32[4,3,2,512]{3,2,1,0:T(2,128)}), f32[4,3,2,512]{3,2,1,0:T(2,128)S(1)}, u32[]{:S(2)}, u32[]{:S(2)}) async-start(f32[4,3,2,512]{3,2,1,0:T(2,128)} %broadcast_in_dim.22), calls=%async_computation | async-start | bytes 98304 | tf_op jit(solution)/shard_map/all_to_all | solution.py:27
  83.7 5.1 %all-to-all-done = f32[4,3,2,512]{3,2,1,0:T(2,128)S(1)} async-done(((f32[4,3,2,512]{3,2,1,0:T(2,128)}), f32[4,3,2,512]{3,2,1,0:T(2,128)S(1)}, u32[]{:S(2)}, u32[]{:S(2)}) %all-to-all-start) | async-done | bytes 49184 | tf_op jit(solution)/shard_map/all_to_all | solution.py:27
  89.8 4.1 %all-to-all-start.1 = ((bf16[4,32,2048]{2,1,0:T(8,128)(2,1)}), bf16[4,32,2048]{2,1,0:T(8,128)(2,1)}, u32[]{:S(2)}, u32[]{:S(2)}) async-start(bf16[4,32,2048]{2,1,0:T(8,128)(2,1)} %broadcast_in_dim.24), calls=%async_computation.1 | async-start | bytes 1048576 | tf_op jit(solution)/shard_map/all_to_all | solution.py:27
  94.6 1.6 pad_maximum_fusion
  96.2 1.9 split.19
  98.0 3.1 split.20
  101.1 2.1 split.18
  103.2 9.4 %concatenate.21 = bf16[2048,1296]{1,0:T(8,128)(2,1)} concatenate(bf16[2048,768]{1,0:T(8,128)(2,1)S(1)} %split.18, bf16[2048,16]{1,0:T(8,128)(2,1)} %split.19, bf16[2048,512]{1,0:T(8,128)(2,1)} %split.20), dimensions={1} | concatenate | bytes 10616832 | tf_op jit(solution)/shard_map/concatenate | solution.py:241
  112.6 5.1 %convolution_convert_fusion.1 = bf16[128,1296]{0,1:T(8,128)(2,1)S(1)} fusion(bf16[128,2048]{1,0:T(8,128)(2,1)} %bitcast.7, bf16[2048,1296]{1,0:T(8,128)(2,1)} %concatenate.21), kind=kOutput, calls=%fused_computation.5 | convolution fusion | flops 679643136 | bytes 6164480 | tf_op jit(solution)/shard_map/dot_general | solution.py:265
  119.1 3.1 collective-permute-start
  122.2 2.7 collective-permute-start.1
  126.6 3.1 collective-permute-done.1
  135.7 1.7 slice-done
  139.0 10.5 %all-to-all-start.2 = ((bf16[64,8,656]{2,1,0:T(8,128)(2,1)}), bf16[64,8,656]{2,1,0:T(8,128)(2,1)S(1)}, u32[]{:S(2)}, u32[]{:S(2)}) async-start(bf16[64,8,656]{2,1,0:T(8,128)(2,1)} %broadcast_in_dim.26), calls=%async_computation.2 | async-start | bytes 1572864 | tf_op jit(solution)/shard_map/all_to_all | solution.py:27
  149.6 24.4 %all_gather.45 = bf16[8,1,8]{2,1,0:T(2,128)(2,1)S(1)} all-gather(bf16[1,1,8]{2,1,0:T(2,128)(2,1)S(1)} %slice.999), channel_id=1, replica_groups=mesh['sp_0'=8,'sp_1'=8,'tp'=4,'dp'=2] {'sp_1'}, dimensions={0}, use_global_device_ids=true | all-gather | bytes 144 | tf_op jit(solution)/shard_map/all_gather | solution.py:68
  174.0 17.4 %all_gather.46 = bf16[8,1,8]{2,1,0:T(2,128)(2,1)S(1)} all-gather(bf16[1,1,8]{2,1,0:T(2,128)(2,1)S(1)} %get-tuple-element.103), channel_id=1, replica_groups=mesh['sp_0'=8,'sp_1'=8,'tp'=4,'dp'=2] {'sp_0'}, dimensions={0}, use_global_device_ids=true | all-gather | bytes 144 | tf_op jit(solution)/shard_map/all_gather | solution.py:68
  191.5 14.7 %all_gather.40 = bf16[8,1,8]{2,1,0:T(2,128)(2,1)S(1)} all-gather(bf16[1,1,8]{2,1,0:T(2,128)(2,1)S(1)} %slice.1000), channel_id=1, replica_groups=mesh['sp_0'=8,'sp_1'=8,'tp'=4,'dp'=2] {'sp_1'}, dimensions={0}, use_global_device_ids=true | all-gather | bytes 144 | tf_op jit(solution)/shard_map/all_gather | solution.py:68
  210.0 14.2 %all_gather.41 = bf16[8,1,8]{2,1,0:T(2,128)(2,1)S(1)} all-gather(bf16[1,1,8]{2,1,0:T(2,128)(2,1)S(1)} %get-tuple-element.83), channel_id=1, replica_groups=mesh['sp_0'=8,'sp_1'=8,'tp'=4,'dp'=2] {'sp_0'}, dimensions={0}, use_global_device_ids=true | all-gather | bytes 144 | tf_op jit(solution)/shard_map/all_gather | solution.py:68
  228.3 3.8 %all-to-all-start.3 = ((bf16[2,256,2048]{2,1,0:T(8,128)(2,1)}), bf16[2,256,2048]{2,1,0:T(8,128)(2,1)S(1)}, u32[]{:S(2)}, u32[]{:S(2)}) async-start(bf16[2,256,2048]{2,1,0:T(8,128)(2,1)} %pad_maximum_fusion), calls=%async_computation.3 | async-start | bytes 4194304 | tf_op jit(solution)/shard_map/all_to_all | solution.py:225
  232.4 2.3 fusion.159
  241.4 1.5 rev.37
  244.2 1.6 copy.104
  246.7 8.3 %rev.35 = bf16[512,512]{1,0:T(8,128)(2,1)} reverse(bf16[512,512]{1,0:T(8,128)(2,1)} %get-tuple-element.48), dimensions={0} | reverse | bytes 1048576 | tf_op jit(solution)/shard_map/jit(_flip)/rev | solution.py:258
  256.3 2.3 fusion.160
  260.8 29.6 %all-gather.12.cloned.1.call-done = bf16[8,1,8,64,128]{4,3,2,1,0:T(8,128)(2,1)} async-done(((bf16[1,1,8,64,128]{4,3,2,1,0:T(8,128)(2,1)}), bf16[8,1,8,64,128]{4,3,2,1,0:T(8,128)(2,1)}) %all-gather.12.cloned.1.call-update) | async-done | bytes 1048592 | tf_op jit(solution)/shard_map/all_gather | solution.py:68
  290.5 3.7 %fusion.13 = f32[1,128,1,8,64]{1,4,3,2,0:T(8,128)} fusion(bf16[512,8,64]{0,2,1:T(8,128)(2,1)} %multiply_convert_fusion.1, f32[512,8]{0,1:T(8,128)S(1)} %subtract_exponential_fusion, bf16[8,1,8,64,128]{4,3,2,1,0:T(8,128)(2,1)} %all-gather.12.cloned.1.call-done, bf16[512,128]{1,0:T(8,128)(2,1)} %rev.37, f32[8]{0:T(128)} %get-tuple-element.95, ...), kind=kOutput, calls=%fused_computation.28 | convolution fusion | flops 88932352 | bytes 3068528 | tf_op jit(solution)/shard_map/clgn,cghpn->clghp/dot_general | solution.py:180
  295.8 36.5 %all-gather.10.cloned.1.call-done = bf16[8,1,8,64,128]{4,3,2,1,0:T(8,128)(2,1)} async-done(((bf16[1,1,8,64,128]{4,3,2,1,0:T(8,128)(2,1)}), bf16[8,1,8,64,128]{4,3,2,1,0:T(8,128)(2,1)}) %all-gather.10.cloned.1.call-update) | async-done | bytes 1048592 | tf_op jit(solution)/shard_map/all_gather | solution.py:68
  332.4 3.4 fusion.12
  338.7 12.1 %all_to_all.25 = bf16[4,32,2048]{2,1,0:T(8,128)(2,1)S(1)} all-to-all(bf16[4,32,2048]{2,1,0:T(8,128)(2,1)S(1)} %bitcast.497), channel_id=1, replica_groups=mesh['sp_0'=8,'sp_1'=8,'tp'=4,'dp'=2] {'tp'}, dimensions={0} | all-to-all | bytes 1048576 | tf_op jit(solution)/shard_map/all_to_all | solution.py:90
  (209 shorter events, 41.0 us)
Async XLA Ops:
  6.5 89.6 %all-gather.8.cloned.1.call-start = ((), (), s32[]{:S(2)}) async-start(), calls=%async_computation.5 | async-start | bytes 8650752 | tf_op jit(solution)/shard_map/all_gather | solution.py:40
  13.1 70.2 %copy-start.6 = (bf16[1,32,2048]{2,1,0:T(8,128)(2,1)S(1)}, bf16[1,32,2048]{2,1,0:T(8,128)(2,1)}, u32[]{:S(2)}) copy-start(bf16[1,32,2048]{2,1,0:T(8,128)(2,1)} %param.17) | copy-start | bytes 393220
  13.1 70.3 %copy-start.41 = (f32[2,8]{1,0:T(2,128)S(1)}, f32[2,8]{1,0:T(2,128)}, u32[]{:S(2)}) copy-start(f32[2,8]{1,0:T(2,128)} %param.31) | copy-start | bytes 196
  13.1 70.4 %copy-start.12 = (bf16[1,8,2048]{2,1,0:T(8,128)(2,1)S(1)}, bf16[1,8,2048]{2,1,0:T(8,128)(2,1)}, u32[]{:S(2)}) copy-start(bf16[1,8,2048]{2,1,0:T(8,128)(2,1)} %param.19) | copy-start | bytes 98308
  13.1 70.5 %copy-start.23 = (bf16[2048]{0:T(1024)(128)(2,1)S(1)}, bf16[2048]{0:T(1024)(128)(2,1)}, u32[]{:S(2)}) copy-start(bf16[2048]{0:T(1024)(128)(2,1)} %param.22) | copy-start | bytes 12292
  13.1 70.5 %copy-start.14 = (bf16[3,512]{1,0:T(4,128)(2,1)S(1)}, bf16[3,512]{1,0:T(4,128)(2,1)}, u32[]{:S(2)}) copy-start(bf16[3,512]{1,0:T(4,128)(2,1)} %param.28) | copy-start | bytes 9220
  13.1 70.5 %copy-start.26 = (bf16[3,128]{1,0:T(4,128)(2,1)S(1)}, bf16[3,128]{1,0:T(4,128)(2,1)}, u32[]{:S(2)}) copy-start(bf16[3,128]{1,0:T(4,128)(2,1)} %param.29) | copy-start | bytes 2308
  13.1 70.5 %copy-start.39 = (bf16[3,128]{1,0:T(4,128)(2,1)S(1)}, bf16[3,128]{1,0:T(4,128)(2,1)}, u32[]{:S(2)}) copy-start(bf16[3,128]{1,0:T(4,128)(2,1)} %param.30) | copy-start | bytes 2308
  13.2 81.4 %copy-start.4 = (bf16[256,2048]{1,0:T(8,128)(2,1)S(1)}, bf16[256,2048]{1,0:T(8,128)(2,1)}, u32[]{:S(2)}) copy-start(bf16[256,2048]{1,0:T(8,128)(2,1)} %param.33) | copy-start | bytes 3145732
  79.0 9.8 %all-to-all-start = ((f32[4,3,2,512]{3,2,1,0:T(2,128)}), f32[4,3,2,512]{3,2,1,0:T(2,128)S(1)}, u32[]{:S(2)}, u32[]{:S(2)}) async-start(f32[4,3,2,512]{3,2,1,0:T(2,128)} %broadcast_in_dim.22), calls=%async_computation | async-start | bytes 98304 | tf_op jit(solution)/shard_map/all_to_all | solution.py:27
  83.4 34.3 %copy-start.21 = (f32[8]{0:T(128)}, f32[8]{0:T(128)S(1)}, u32[]{:S(2)}) copy-start(f32[8]{0:T(128)S(1)} %get-tuple-element.112) | copy-start | bytes 100
  83.4 34.5 %copy-start.19 = (f32[8]{0:T(128)}, f32[8]{0:T(128)S(1)}, u32[]{:S(2)}) copy-start(f32[8]{0:T(128)S(1)} %get-tuple-element.113) | copy-start | bytes 100
  89.8 22.8 %all-to-all-start.1 = ((bf16[4,32,2048]{2,1,0:T(8,128)(2,1)}), bf16[4,32,2048]{2,1,0:T(8,128)(2,1)}, u32[]{:S(2)}, u32[]{:S(2)}) async-start(bf16[4,32,2048]{2,1,0:T(8,128)(2,1)} %broadcast_in_dim.24), calls=%async_computation.1 | async-start | bytes 1048576 | tf_op jit(solution)/shard_map/all_to_all | solution.py:27
  94.0 138.3 %all-gather.16.cloned.1.call-start = ((), (), s32[]{:S(2)}) async-start(), calls=%async_computation.9 | async-start | bytes 1179648 | tf_op jit(solution)/shard_map/all_gather | solution.py:68
  117.7 12.9 %copy-start.1 = (bf16[128,1296]{0,1:T(8,128)(2,1)}, bf16[128,1296]{0,1:T(8,128)(2,1)S(1)}, u32[]{:S(2)}) copy-start(bf16[128,1296]{0,1:T(8,128)(2,1)S(1)} %convolution_convert_fusion.1) | copy-start | bytes 995332
  119.1 7.6 %collective-permute-start = (bf16[1,768]{0,1:T(8,128)(2,1)S(1)}, bf16[1,768]{0,1:T(8,128)(2,1)S(1)}, u32[]{:S(2)}, u32[]{:S(2)}) collective-permute-start(bf16[1,768]{0,1:T(8,128)(2,1)S(1)} %get-tuple-element.49), channel_id=1, source_target_pairs={{0,8},{8,16},{16,24},{24,32},{32,40},{40,48},{48,56},{56,64},{64,7... | collective-permute-start | bytes 4616 | tf_op jit(solution)/shard_map/ppermute | solution.py:50
  122.2 7.6 %collective-permute-start.1 = (bf16[1,768]{0,1:T(8,128)(2,1)S(1)}, bf16[1,768]{0,1:T(8,128)(2,1)S(1)}, u32[]{:S(2)}, u32[]{:S(2)}) collective-permute-start(bf16[1,768]{0,1:T(8,128)(2,1)S(1)} %get-tuple-element.50), channel_id=1, source_target_pairs={{8,0},{16,8},{24,16},{32,24},{40,32},{48,40},{56,48},{64,56},{72,6... | collective-permute-start | bytes 4616 | tf_op jit(solution)/shard_map/ppermute | solution.py:51
  139.0 89.2 %all-to-all-start.2 = ((bf16[64,8,656]{2,1,0:T(8,128)(2,1)}), bf16[64,8,656]{2,1,0:T(8,128)(2,1)S(1)}, u32[]{:S(2)}, u32[]{:S(2)}) async-start(bf16[64,8,656]{2,1,0:T(8,128)(2,1)} %broadcast_in_dim.26), calls=%async_computation.2 | async-start | bytes 1572864 | tf_op jit(solution)/shard_map/all_to_all | solution.py:27
  149.5 106.8 %all-gather.14.cloned.1.call-start = ((), (), s32[]{:S(2)}) async-start(), calls=%async_computation.8 | async-start | bytes 1179648 | tf_op jit(solution)/shard_map/all_gather | solution.py:68
  174.0 58.3 %copy-start.31 = (f32[8]{0:T(128)}, f32[8]{0:T(128)S(1)}, u32[]{:S(2)}) copy-start(f32[8]{0:T(128)S(1)} %get-tuple-element.104) | copy-start | bytes 100
  174.0 58.3 %copy-start.32 = (f32[8]{0:T(128)}, f32[8]{0:T(128)S(1)}, u32[]{:S(2)}) copy-start(f32[8]{0:T(128)S(1)} %get-tuple-element.105) | copy-start | bytes 100
  174.0 58.3 %copy-start.33 = (f32[8]{0:T(128)}, f32[8]{0:T(128)S(1)}, u32[]{:S(2)}) copy-start(f32[8]{0:T(128)S(1)} %get-tuple-element.106) | copy-start | bytes 100
  174.0 58.3 %copy-start.34 = (f32[8]{0:T(128)}, f32[8]{0:T(128)S(1)}, u32[]{:S(2)}) copy-start(f32[8]{0:T(128)S(1)} %get-tuple-element.107) | copy-start | bytes 100
  174.0 58.3 %copy-start.35 = (f32[8]{0:T(128)}, f32[8]{0:T(128)S(1)}, u32[]{:S(2)}) copy-start(f32[8]{0:T(128)S(1)} %get-tuple-element.108) | copy-start | bytes 100
  174.0 58.3 %copy-start.36 = (f32[8]{0:T(128)}, f32[8]{0:T(128)S(1)}, u32[]{:S(2)}) copy-start(f32[8]{0:T(128)S(1)} %get-tuple-element.109) | copy-start | bytes 100
  174.0 58.3 %copy-start.37 = (f32[8]{0:T(128)}, f32[8]{0:T(128)S(1)}, u32[]{:S(2)}) copy-start(f32[8]{0:T(128)S(1)} %get-tuple-element.110) | copy-start | bytes 100
  174.0 58.3 %copy-start.38 = (f32[8]{0:T(128)}, f32[8]{0:T(128)S(1)}, u32[]{:S(2)}) copy-start(f32[8]{0:T(128)S(1)} %get-tuple-element.111) | copy-start | bytes 100
  228.3 109.9 %all-to-all-start.3 = ((bf16[2,256,2048]{2,1,0:T(8,128)(2,1)}), bf16[2,256,2048]{2,1,0:T(8,128)(2,1)S(1)}, u32[]{:S(2)}, u32[]{:S(2)}) async-start(bf16[2,256,2048]{2,1,0:T(8,128)(2,1)} %pad_maximum_fusion), calls=%async_computation.3 | async-start | bytes 4194304 | tf_op jit(solution)/shard_map/all_to_all | solution.py:225
  232.1 58.4 %all-gather.12.cloned.1.call-start = ((), (), s32[]{:S(2)}) async-start(), calls=%async_computation.7 | async-start | bytes 1179648 | tf_op jit(solution)/shard_map/all_gather | solution.py:68
  234.7 97.7 %all-gather.10.cloned.1.call-start = ((), (), s32[]{:S(2)}) async-start(), calls=%async_computation.6 | async-start | bytes 1179648 | tf_op jit(solution)/shard_map/all_gather | solution.py:68
  246.7 9.6 %copy-start.30 = (f32[8]{0:T(128)S(1)}, f32[8]{0:T(128)}, u32[]{:S(2)}) copy-start(f32[8]{0:T(128)} %get-tuple-element.85) | copy-start | bytes 100
  290.4 41.9 %copy-start.5 = (bf16[512,8,64]{0,2,1:T(8,128)(2,1)S(1)}, bf16[512,8,64]{0,2,1:T(8,128)(2,1)}, u32[]{:S(2)}) copy-start(bf16[512,8,64]{0,2,1:T(8,128)(2,1)} %multiply_convert_fusion.2) | copy-start | bytes 1572868
  (25 other events, 102.0 us)
Sparse Core Ops, SparseCore 0:
  13.3 28.6 all-gather.7
  132.9 42.1 all-gather.15
  209.5 37.9 all-gather.13
  249.5 40.9 all-gather.11
  292.4 39.9 all-gather.9
